TPU v7x, 32 devices: a whole 2x2x4 slice. The times are simulated.
32 devices in a mesh: sp: 16 (over z, y, x), tp: 2 (over core).
Axes of the slice: x: 2, y: 2, z: 4, core: 2. Of those that a mesh axis runs over, the one named last changes fastest.
Arguments:
- residual_in: bfloat16 [6144, 2048], P(('sp', 'tp')), may hold values from -6 to 6
- conv_values: bfloat16 [6144, 1024], P('sp', 'tp'), may hold values from -60 to 60
- conv_gates: bfloat16 [6144, 1024], P('sp', 'tp'), may hold values from -8 to 8
- conv_kernel: float32 [31, 1024], P(None, 'tp'), may hold values from -1 to 1
- conv_bias: float32 [1024], P('tp'), may hold values from -3 to 3
- chan_gain: float32 [1024], P('tp'), may hold values from 0.1 to 1.9
- chan_shift: float32 [1024], P('tp'), may hold values from -3 to 3
- out_weight: bfloat16 [1024, 2048], replicated, may hold values from -0.1875 to 0.1875
- norm_gain: float32 [2048], replicated, may hold values from 0.1 to 1.9
- route_ids: int32 [6144, 2], P(('sp', 'tp')), may hold values from 0 to 15, all different within a row; in each aligned block of 192 rows (0 to 191, 192 to 383, ...) at most 48 rows name the same one
- route_weights: float32 [6144, 2], P(('sp', 'tp')), may hold values from 0.25 to 1.5
- expert_gate: bfloat16 [16, 2048, 2048], P('sp', None, 'tp'), may hold values from -0.125 to 0.125
- expert_up: bfloat16 [16, 2048, 2048], P('sp', None, 'tp'), may hold values from -0.125 to 0.125
- expert_down: bfloat16 [16, 2048, 2048], P('sp', 'tp'), may hold values from -0.125 to 0.125
Outputs:
- layer_out: bfloat16 [6144, 2048], P(('sp', 'tp'))
Inputs may be any that keep to these rules, and one draw needn't show every extreme that they name: `route_ids`: each row names 2 different experts. Among the rows of one device (aligned blocks of 192 rows) no expert is named by more than 48 rows, a bound that some block reaches.
All inputs are finite; a program needn't handle non-finite values.
Results may differ from a plain program's by a relative error of at most 0.014.
Values may be sent and summed in bfloat16 or wider, within the bound.
A program may use at most 128 MiB of HBM per device.

v0:
```python
import jax
import jax.numpy as jnp
from jax import lax
from jax.sharding import PartitionSpec as P


def from_behind(value, axis, steps):
    count = lax.axis_size(axis)
    first, last = (max(0, -steps), min(count, count - steps))
    return lax.ppermute(value, axis, [(source, source + steps) for source in range(first, last)])


def on_device(
    residual_in,
    conv_values,
    conv_gates,
    conv_kernel,
    conv_bias,
    chan_gain,
    chan_shift,
    out_weight,
    norm_gain,
    route_ids,
    route_weights,
    expert_gate,
    expert_up,
    expert_down,
):
    taps_count = conv_kernel.shape[0]
    tok_count, local_chan = conv_values.shape
    tp_count = lax.axis_size("tp")
    all_chan = local_chan * tp_count
    gated = (
        conv_values.astype(jnp.float32) * jax.nn.sigmoid(conv_gates.astype(jnp.float32))
    ).astype(jnp.bfloat16)
    earlier = from_behind(gated[tok_count - (taps_count - 1) :], "sp", 1)
    extended = jnp.concatenate([earlier, gated], 0).astype(jnp.float32)
    mixed = jnp.zeros((tok_count, local_chan), jnp.float32) + conv_bias[None, :]
    for tap_index in range(taps_count):
        mixed = (
            mixed + conv_kernel[tap_index][None, :] * extended[tap_index : tap_index + tok_count]
        )
    row_total = jnp.sum(mixed, 1)
    row_square = jnp.sum(mixed * mixed, 1)
    row_total, row_square = lax.psum((row_total, row_square), "tp")
    center = (row_total / all_chan)[:, None]
    spread = (row_square / all_chan)[:, None] - center * center
    normed = (mixed - center) * lax.rsqrt(spread + 1e-06) * chan_gain[None, :] + chan_shift[None, :]
    activated = jax.nn.silu(normed).astype(jnp.bfloat16)
    row_count = tok_count // tp_count
    regrouped = lax.all_to_all(activated, "tp", split_axis=0, concat_axis=1, tiled=True)
    projected = jnp.dot(regrouped, out_weight, preferred_element_type=jnp.float32)
    after_f = (residual_in.astype(jnp.float32) + projected).astype(jnp.bfloat16).astype(jnp.float32)
    normal_rows = (
        after_f
        * lax.rsqrt(jnp.mean(after_f * after_f, 1, keepdims=True) + 1e-06)
        * norm_gain[None, :]
    ).astype(jnp.bfloat16)
    model_width = normal_rows.shape[1]
    experts_all = expert_gate.shape[0] * lax.axis_size("sp")
    choose_count = route_ids.shape[1]
    slot_cap = max(2, (2 * choose_count * row_count + experts_all - 1) // experts_all)
    onehot = (
        route_ids.reshape(-1)[:, None] == jnp.arange(experts_all, dtype=jnp.int32)[None, :]
    ).astype(jnp.int32)
    before = jnp.cumsum(onehot, 0) - onehot
    ranking = jnp.sum(before * onehot, 1).reshape(row_count, choose_count)
    slot_ids = route_ids * slot_cap + ranking
    positions = lax.broadcasted_iota(jnp.int32, (experts_all * slot_cap, 1, 1), 0)
    dispatch = jnp.any(positions == slot_ids[None, :, :], axis=2).astype(jnp.bfloat16)
    sendable = jnp.dot(dispatch, normal_rows, preferred_element_type=jnp.float32).astype(
        jnp.bfloat16
    )
    sendable = sendable.reshape(experts_all, slot_cap, model_width)
    both_rows = lax.all_gather(
        lax.all_to_all(sendable, "sp", split_axis=0, concat_axis=0, tiled=True),
        "tp",
        axis=0,
        tiled=True,
    )
    leading, slot_width, widths = both_rows.shape
    flat_rows = both_rows.reshape(leading * slot_width, widths)
    gate = jnp.dot(flat_rows, expert_gate[0], preferred_element_type=jnp.float32)
    upper = jnp.dot(flat_rows, expert_up[0], preferred_element_type=jnp.float32)
    hidden = (jax.nn.silu(gate) * upper).astype(jnp.bfloat16)
    summed = lax.psum_scatter(
        jnp.dot(hidden, expert_down[0], preferred_element_type=jnp.float32)
        .reshape(leading, slot_width, widths)
        .astype(jnp.bfloat16),
        "tp",
        scatter_dimension=0,
        tiled=True,
    )
    results = lax.all_to_all(summed, "sp", split_axis=0, concat_axis=0, tiled=True)
    flat_out = results.reshape(experts_all * slot_cap, model_width)
    picked = (
        jnp.take(flat_out, slot_ids.reshape(-1), axis=0)
        .reshape(row_count, choose_count, model_width)
        .astype(jnp.float32)
    )
    combined = after_f + jnp.sum(route_weights[:, :, None] * picked, 1)
    return combined.astype(jnp.bfloat16)


def solution(mesh):
    placed = (
        P(("sp", "tp"), None),
        P("sp", "tp"),
        P("sp", "tp"),
        P(None, "tp"),
        P("tp"),
        P("tp"),
        P("tp"),
        P(),
        P(),
        P(("sp", "tp"), None),
        P(("sp", "tp"), None),
        P("sp", None, "tp"),
        P("sp", None, "tp"),
        P("sp", "tp", None),
    )
    return jax.shard_map(
        on_device, mesh=mesh, in_specs=placed, out_specs=P(("sp", "tp"), None), check_vma=False
    )
```

profile of v0, /device:TPU:14, one launch (start us, length us, event | category | flops | bytes accessed | tf_op | source)
XLA Modules:
  0.0 266.2 jit_solution(6359469079230641675)
XLA Ops:
  6.5 1.3 multiply_convert_fusion.4
  7.9 3.4 %collective-permute-start = (bf16[30,512]{1,0:T(8,128)(2,1)S(1)}, bf16[30,512]{1,0:T(8,128)(2,1)S(1)}, u32[]{:S(2)}, u32[]{:S(2)}) collective-permute-start(bf16[30,512]{1,0:T(8,128)(2,1)S(1)} %slice.262), channel_id=1, source_target_pairs={{0,2},{2,4},{4,6},{6,8},{8,10},{10,12},{12,14},{14,16},{16,18},{18... | collective-permute-start | bytes 92168 | tf_op jit(solution)/shard_map/ppermute | solution.py:10
  11.3 1.2 fusion.47
  12.5 1.0 fusion.48
  13.5 0.8 copy.42
  14.3 0.1 eq.42
  14.4 0.1 eq.38
  14.6 0.9 reduce-window.6
  15.5 0.2 slice_reduce_fusion
  15.7 0.1 fusion.42
  15.8 0.1 reshape.98
  16.0 0.1 copy.45
  16.1 0.7 compare_and_fusion
  16.8 0.2 fusion.6
  16.9 0.0 collective-permute-done
  16.9 0.1 maximum_convert_fusion
  17.1 0.0 copy-start.4
  17.1 0.0 copy-start.5
  17.1 3.8 %fusion.45 = (f32[384]{0:T(512)S(1)}, f32[384]{0:T(512)S(1)}, f32[384,512]{1,0:T(8,128)S(1)}) fusion(f32[414,512]{1,0:T(8,128)S(1)} %maximum_convert_fusion, f32[512]{0:T(512)S(1)} %bitcast.110, f32[512]{0:T(512)S(1)} %bitcast.111, f32[512]{0:T(512)S(1)} %bitcast.82, f32[512]{0:T(512)S(1)} %bitcast.83, f32[512]{0:T(512)S(1)} %bitcast.84, ...), kind=kLoop, calls=%fused_computation.104 | loop fusion | flops 12778752 | bytes 25234432 | tf_op jit(solution)/shard_map/reduce_sum | solution.py:43
  20.9 0.0 copy-start.2
  20.9 2.6 all-reduce
  23.6 0.4 multiply_convert_fusion.3
  23.9 4.0 %all_to_all.29 = bf16[2,192,512]{2,1,0:T(8,128)(2,1)S(1)} all-to-all(bf16[2,192,512]{2,1,0:T(8,128)(2,1)S(1)} %bitcast.79), channel_id=1, replica_groups=mesh['sp'=16,'tp'=2] {'tp'}, dimensions={0} | all-to-all | bytes 786432 | tf_op jit(solution)/shard_map/all_to_all | solution.py:51
  28.0 0.0 copy-start.3
  28.0 3.3 %multiply_reduce_fusion.1 = (f32[192]{0:T(256)S(1)}, f32[192,2048]{1,0:T(8,128)S(1)}) fusion(bf16[192,1024]{1,0:T(8,128)(2,1)S(1)} %bitcast.77, bf16[1024,2048]{1,0:T(8,128)(2,1)} %param.21, bf16[192,2048]{1,0:T(8,128)(2,1)S(1)} %copy-done.2), kind=kOutput, calls=%fused_computation.15 | convolution fusion | flops 807665472 | bytes 6947584 | tf_op jit(solution)/shard_map/dot_general | solution.py:52
  31.4 1.2 copy-done
  32.6 1.1 convolution_convert_fusion.1
  33.7 75.6 %all_to_all.30 = bf16[16,48,2048]{2,1,0:T(8,128)(2,1)} all-to-all(bf16[16,48,2048]{2,1,0:T(8,128)(2,1)S(1)} %bitcast.76), channel_id=1, replica_groups=mesh['sp'=16,'tp'=2] {'sp'}, dimensions={0} | all-to-all | bytes 6291456 | tf_op jit(solution)/shard_map/all_to_all | solution.py:76
  109.3 0.0 all-gather.2.cloned.1.call-update
  109.3 0.2 reduce-scatter.2.cloned.1.call-start
  109.5 16.9 %all-gather.2.cloned.1.call-done = bf16[32,48,2048]{2,1,0:T(8,128)(2,1)} async-done(((bf16[16,48,2048]{2,1,0:T(8,128)(2,1)}), bf16[32,48,2048]{2,1,0:T(8,128)(2,1)}) %all-gather.2.cloned.1.call-update) | async-done | bytes 6291472 | tf_op jit(solution)/shard_map/all_gather | solution.py:75
  126.4 10.1 %fusion.2 = f32[1536,1024]{1,0:T(8,128)S(1)} fusion(bf16[1536,2048]{1,0:T(8,128)(2,1)} %bitcast.112, bf16[1,2048,1024]{2,1,0:T(8,128)(2,1)} %param.25), kind=kOutput, calls=%fused_computation.5 | convolution fusion | flops 6442450944 | bytes 16777216 | tf_op jit(solution)/shard_map/dot_general | solution.py:83
  136.6 0.0 copy-start.10
  136.6 7.4 %multiply_convert_fusion = bf16[1536,1024]{1,0:T(8,128)(2,1)S(1)} fusion(f32[1536,1024]{1,0:T(8,128)S(1)} %fusion.2, bf16[1536,2048]{1,0:T(8,128)(2,1)S(1)} %bitcast.113, bf16[1,2048,1024]{2,1,0:T(8,128)(2,1)S(1)} %copy-done.9), kind=kOutput, calls=%fused_computation.1 | convolution fusion | flops 6451888128 | bytes 19922944 | tf_op jit(solution)/shard_map/dot_general | solution.py:84
  144.1 8.8 %convolution_convert_fusion = bf16[32,48,2048]{2,1,0:T(8,128)(2,1)} fusion(bf16[32,48,1024]{2,1,0:T(8,128)(2,1)S(1)} %bitcast.114, bf16[1,1024,2048]{2,1,0:T(8,128)(2,1)S(1)} %copy-done.10), kind=kOutput, calls=%fused_computation.2 | convolution fusion | flops 6445596672 | bytes 13631488 | tf_op jit(solution)/shard_map/dot_general | solution.py:87
  152.8 0.0 reduce-scatter.2.cloned.1.call-update
  152.9 0.0 copy-start.6
  152.9 16.2 %reduce-scatter.2.cloned.1.call-done = bf16[16,48,2048]{2,1,0:T(8,128)(2,1)} async-done(((bf16[32,48,2048]{2,1,0:T(8,128)(2,1)}), bf16[16,48,2048]{2,1,0:T(8,128)(2,1)}) %reduce-scatter.2.cloned.1.call-update) | async-done | bytes 3145744 | tf_op jit(solution)/shard_map/reduce_scatter | solution.py:86
  169.1 7.0 %all-to-all-start.2 = ((bf16[16,48,2048]{2,1,0:T(8,128)(2,1)}), bf16[16,48,2048]{2,1,0:T(8,128)(2,1)S(1)}, u32[]{:S(2)}, u32[]{:S(2)}) async-start(bf16[16,48,2048]{2,1,0:T(8,128)(2,1)} %reduce-scatter.2.cloned.1.call-done), calls=%async_computation.3 | async-start | bytes 6291456 | tf_op jit(solution)/shard_map/all_to_all | solution.py:94
  176.0 0.1 copy.47
  176.2 0.1 reshape.102
  176.3 0.2 copy.46
  176.5 0.1 copy.41
  176.6 69.5 %all-to-all-done.2 = bf16[16,48,2048]{2,1,0:T(8,128)(2,1)S(1)} async-done(((bf16[16,48,2048]{2,1,0:T(8,128)(2,1)}), bf16[16,48,2048]{2,1,0:T(8,128)(2,1)S(1)}, u32[]{:S(2)}, u32[]{:S(2)}) %all-to-all-start.2) | async-done | bytes 3145760 | tf_op jit(solution)/shard_map/all_to_all | solution.py:94
  246.1 3.1 %gather_fusion = bf16[384,2048]{1,0:T(8,128)(2,1)} fusion(bf16[768,2048]{1,0:T(8,128)(2,1)S(1)} %bitcast.75, s32[1024]{0:T(1024)S(1)} %pad_clamp_fusion), kind=kCustom, calls=%fused_computation | custom fusion | bytes 3147264 | tf_op jit(solution)/shard_map/jit(_take)/gather | solution.py:97
  249.2 2.9 %gather.7 = bf16[192,2,2048]{2,1,0:T(2,128)(2,1)S(1)} reshape(bf16[384,2048]{1,0:T(8,128)(2,1)} %gather_fusion) | data formatting | bytes 3145728 | tf_op jit(solution)/shard_map/jit(_take)/gather | solution.py:97
  252.1 6.1 %multiply_reduce_fusion = f32[192,2048]{1,0:T(8,128)S(1)} fusion(bf16[192,2,2048]{2,1,0:T(2,128)(2,1)S(1)} %gather.7, pred[192,2]{1,0:T(8,128)(4,1)S(1)} %copy.46, f32[192,2]{1,0:T(8,128)S(1)} %copy.41), kind=kLoop, calls=%fused_computation.8 | loop fusion | flops 2752512 | bytes 3147648 | tf_op jit(solution)/shard_map/reduce_sum | solution.py:101
  258.3 1.1 add_convert_fusion
  (24 shorter events, 0.2 us)
Async XLA Ops:
  6.5 10.5 %copy-start.7 = (f32[512]{0:T(512)S(1)}, f32[512]{0:T(512)}, u32[]{:S(2)}) copy-start(f32[512]{0:T(512)} %param.18) | copy-start | bytes 6148
  6.5 119.9 %all-gather.2.cloned.1.call-start = ((), (), s32[]{:S(2)}) async-start(), calls=%async_computation.4 | async-start | bytes 9437184 | tf_op jit(solution)/shard_map/all_gather | solution.py:75
  7.9 9.0 %collective-permute-start = (bf16[30,512]{1,0:T(8,128)(2,1)S(1)}, bf16[30,512]{1,0:T(8,128)(2,1)S(1)}, u32[]{:S(2)}, u32[]{:S(2)}) collective-permute-start(bf16[30,512]{1,0:T(8,128)(2,1)S(1)} %slice.262), channel_id=1, source_target_pairs={{0,2},{2,4},{4,6},{6,8},{8,10},{10,12},{12,14},{14,16},{16,18},{18... | collective-permute-start | bytes 92168 | tf_op jit(solution)/shard_map/ppermute | solution.py:10
  17.1 6.5 %copy-start.4 = (f32[512]{0:T(512)S(1)}, f32[512]{0:T(512)}, u32[]{:S(2)}) copy-start(f32[512]{0:T(512)} %param.20) | copy-start | bytes 6148
  17.1 6.5 %copy-start.5 = (f32[512]{0:T(512)S(1)}, f32[512]{0:T(512)}, u32[]{:S(2)}) copy-start(f32[512]{0:T(512)} %param.19) | copy-start | bytes 6148
  20.9 7.1 %copy-start.2 = (bf16[192,2048]{1,0:T(8,128)(2,1)S(1)}, bf16[192,2048]{1,0:T(8,128)(2,1)}, u32[]{:S(2)}) copy-start(bf16[192,2048]{1,0:T(8,128)(2,1)} %param.14) | copy-start | bytes 2359300
  28.0 4.5 %copy-start.3 = (f32[2048]{0:T(1024)S(1)}, f32[2048]{0:T(1024)}, u32[]{:S(2)}) copy-start(f32[2048]{0:T(1024)} %param.22) | copy-start | bytes 24580
  31.4 1.2 copy-start
  109.3 59.8 %reduce-scatter.2.cloned.1.call-start = ((), (), s32[]{:S(2)}) async-start(), calls=%async_computation.5 | async-start | bytes 9437184 | tf_op jit(solution)/shard_map/reduce_scatter | solution.py:86
  126.4 10.1 %copy-start.8 = (bf16[32,48,2048]{2,1,0:T(8,128)(2,1)S(1)}, bf16[32,48,2048]{2,1,0:T(8,128)(2,1)}, u32[]{:S(2)}) copy-start(bf16[32,48,2048]{2,1,0:T(8,128)(2,1)} %all-gather.2.cloned.1.call-done) | copy-start | bytes 18874372
  126.4 10.1 %copy-start.9 = (bf16[1,2048,1024]{2,1,0:T(8,128)(2,1)S(1)}, bf16[1,2048,1024]{2,1,0:T(8,128)(2,1)}, u32[]{:S(2)}) copy-start(bf16[1,2048,1024]{2,1,0:T(8,128)(2,1)} %param.26) | copy-start | bytes 12582916
  136.6 7.5 %copy-start.10 = (bf16[1,1024,2048]{2,1,0:T(8,128)(2,1)S(1)}, bf16[1,1024,2048]{2,1,0:T(8,128)(2,1)}, u32[]{:S(2)}) copy-start(bf16[1,1024,2048]{2,1,0:T(8,128)(2,1)} %param.27) | copy-start | bytes 12582916
  152.9 23.6 %copy-start.6 = (f32[192,2]{0,1:T(2,128)S(1)}, f32[192,2]{0,1:T(2,128)}, u32[]{:S(2)}) copy-start(f32[192,2]{0,1:T(2,128)} %param.24) | copy-start | bytes 4612
  169.1 77.0 %all-to-all-start.2 = ((bf16[16,48,2048]{2,1,0:T(8,128)(2,1)}), bf16[16,48,2048]{2,1,0:T(8,128)(2,1)S(1)}, u32[]{:S(2)}, u32[]{:S(2)}) async-start(bf16[16,48,2048]{2,1,0:T(8,128)(2,1)} %reduce-scatter.2.cloned.1.call-done), calls=%async_computation.3 | async-start | bytes 6291456 | tf_op jit(solution)/shard_map/all_to_all | solution.py:94
  249.2 9.0 %copy-start.1 = (f32[192,2048]{1,0:T(8,128)S(1)}, f32[192,2048]{1,0:T(8,128)}, u32[]{:S(2)}) copy-start(f32[192,2048]{1,0:T(8,128)} %copy-done) | copy-start | bytes 4718596
Sparse Core Ops, SparseCore 0:
  109.4 16.9 all-gather.1
  153.0 16.0 reduce-scatter.1
where the time goes:
time: 267 us; the launch traced here: 266 us
  waiting for transfers between devices  103 us (39%)
  blocking collectives  82.3 us (31%)
  matrix products  30.7 us (11%)
  other arithmetic  14.8 us (6%)
  between operations  13.7 us (5%)
  local copies, waits for them, and re-layouts  11.5 us (4%)
  starting transfers between devices  10.6 us (4%)
    all_to_all x1, blocking collectives, on_device(): lax.all_to_all(sendable, 'sp', split_axis=0, concat_axis=0, tiled=True)  75.6 us
    all_to_all x1, waiting for transfers between devices, on_device(): lax.all_to_all(summed, 'sp', split_axis=0, concat_axis=0, tiled=True)  69.5 us
    all_gather x1, waiting for transfers between devices, on_device(): lax.all_gather(lax.all_to_all(sendable, 'sp', split_axis=0, concat_axis=0...  16.9 us
    reduce_scatter x1, waiting for transfers between devices, on_device(): lax.psum_scatter(jnp.dot(hidden, expert_down[0], preferred_element_type=j...  16.2 us
    dot_general x1, matrix products, on_device(): jnp.dot(flat_rows, expert_gate[0], preferred_element_type=jnp.float32)  10.1 us
    dot_general x1, matrix products, on_device(): jnp.dot(hidden, expert_down[0], preferred_element_type=jnp.float32)  8.76 us
    dot_general x1, matrix products, on_device(): upper = jnp.dot(flat_rows, expert_up[0], preferred_element_type=jnp.float32)  7.44 us
    all_to_all x1, starting transfers between devices, on_device(): lax.all_to_all(summed, 'sp', split_axis=0, concat_axis=0, tiled=True)  6.96 us
  transfers between devices with their start and end apart: 4, of which 3 were waited for; matrix products, arithmetic and copies ran while one was open for 2% of the time, Pallas kernels for 0%

commit v1 on v0

v1 whole, which is shorter than its diff:
```python
import functools

import jax
import jax.numpy as jnp
from jax import lax
from jax.experimental import pallas as pl
from jax.experimental.pallas import tpu as pltpu
from jax.sharding import PartitionSpec as P

GROUPS = 4
ORDER = (0, 2, 1, 3)
MESH = pl.DeviceIdType.MESH


def flipped(index, offset):
    result, bit = index, 1
    while bit <= offset:
        if offset & bit:
            result = result + bit * (1 - 2 * ((index // bit) % 2))
        bit *= 2
    return result


def experts_kernel(
    count, cap, send, gate_in, up_in, down_in, out,
    rows, part, given, total, hidden, gate_w, up_w, down_w,
    sent, came, back_sent, back_came, pair_sent, pair_came, part_sent, part_came, loaded,
):
    me, other = lax.axis_index("sp"), 1 - lax.axis_index("tp")
    per_group = count // GROUPS
    half = per_group * cap
    loads = [
        pltpu.make_async_copy(source.at[0], target, loaded.at[number])
        for number, (source, target) in enumerate(
            ((gate_in, gate_w), (up_in, up_w), (down_in, down_w))
        )
    ]
    for load in loads:
        load.start()

    barrier = pltpu.get_barrier_semaphore()
    for offset in range(1, count):
        pl.semaphore_signal(
            barrier, inc=1, device_id={"sp": flipped(me, offset)}, device_id_type=MESH
        )
    pl.semaphore_signal(barrier, inc=1, device_id={"tp": other}, device_id_type=MESH)
    pl.semaphore_wait(barrier, count)

    outgoing = {}
    for group in ORDER:
        for place in range(per_group):
            offset = group * per_group + place
            source = send.at[pl.ds(offset * cap, cap)]
            target = rows.at[group, pl.ds(place * cap, cap)]
            if offset == 0:
                copy = pltpu.make_async_copy(source, target, sent.at[0])
            else:
                copy = pltpu.make_async_remote_copy(
                    src_ref=source,
                    dst_ref=target,
                    send_sem=sent.at[offset],
                    recv_sem=came.at[offset],
                    device_id={"sp": flipped(me, offset)},
                    device_id_type=MESH,
                )
            copy.start()
            outgoing[offset] = copy

    late, returning = [], {}
    for turn, group in enumerate(ORDER):
        for place in range(per_group):
            offset = group * per_group + place
            if offset == 0:
                outgoing[0].wait()
            else:
                outgoing[offset].wait_recv()
        pair = pltpu.make_async_remote_copy(
            src_ref=rows.at[group, pl.ds(0, half)],
            dst_ref=rows.at[group, pl.ds(half, half)],
            send_sem=pair_sent.at[group],
            recv_sem=pair_came.at[group],
            device_id={"tp": other},
            device_id_type=MESH,
        )
        pair.start()
        late.append(pair)
        if turn == 0:
            for load in loads:
                load.wait()
        pair.wait_recv()

        wide = min(256, gate_w.shape[1])

        def first(step, carry, group=group):
            columns = pl.ds(pl.multiple_of(step * wide, wide), wide)
            gate = jnp.dot(rows[group], gate_w[:, columns], preferred_element_type=jnp.float32)
            upper = jnp.dot(rows[group], up_w[:, columns], preferred_element_type=jnp.float32)
            hidden[:, columns] = (jax.nn.silu(gate) * upper).astype(jnp.bfloat16)
            return carry

        lax.fori_loop(0, gate_w.shape[1] // wide, first, 0)

        def second(step, carry, group=group):
            columns = pl.ds(pl.multiple_of(step * wide, wide), wide)
            part[group, :, columns] = jnp.dot(
                hidden[...], down_w[:, columns], preferred_element_type=jnp.float32
            ).astype(jnp.bfloat16)
            return carry

        lax.fori_loop(0, down_w.shape[1] // wide, second, 0)

        share = pltpu.make_async_remote_copy(
            src_ref=part.at[group, pl.ds(half, half)],
            dst_ref=given.at[group],
            send_sem=part_sent.at[group],
            recv_sem=part_came.at[group],
            device_id={"tp": other},
            device_id_type=MESH,
        )
        share.start()
        late.append(share)
        share.wait_recv()
        total[group] = (
            part[group, pl.ds(0, half)].astype(jnp.float32) + given[group].astype(jnp.float32)
        ).astype(jnp.bfloat16)
        for place in range(per_group):
            offset = group * per_group + place
            source = total.at[group, pl.ds(place * cap, cap)]
            target = out.at[pl.ds(offset * cap, cap)]
            if offset == 0:
                copy = pltpu.make_async_copy(source, target, back_sent.at[0])
            else:
                copy = pltpu.make_async_remote_copy(
                    src_ref=source,
                    dst_ref=target,
                    send_sem=back_sent.at[offset],
                    recv_sem=back_came.at[offset],
                    device_id={"sp": flipped(me, offset)},
                    device_id_type=MESH,
                )
            copy.start()
            returning[offset] = copy

    for offset in range(1, count):
        outgoing[offset].wait_send()
    for copy in late:
        copy.wait_send()
    for offset in range(count):
        returning[offset].wait()


def run_experts(sendable, expert_gate, expert_up, expert_down, count, cap):
    width, units = expert_gate.shape[1], expert_gate.shape[2]
    half = count // GROUPS * cap
    grouped = pltpu.SemaphoreType.DMA((GROUPS,))
    each = pltpu.SemaphoreType.DMA((count,))
    vmem = pl.BlockSpec(memory_space=pltpu.VMEM)
    anywhere = pl.BlockSpec(memory_space=pl.ANY)
    held = jnp.bfloat16
    return pl.pallas_call(
        functools.partial(experts_kernel, count, cap),
        out_shape=jax.ShapeDtypeStruct(sendable.shape, held),
        in_specs=[vmem, anywhere, anywhere, anywhere],
        out_specs=vmem,
        scratch_shapes=[
            pltpu.VMEM((GROUPS, 2 * half, width), held),
            pltpu.VMEM((GROUPS, 2 * half, width), held),
            pltpu.VMEM((GROUPS, half, width), held),
            pltpu.VMEM((GROUPS, half, width), held),
            pltpu.VMEM((2 * half, units), held),
            pltpu.VMEM((width, units), held),
            pltpu.VMEM((width, units), held),
            pltpu.VMEM((units, width), held),
            each, each, each, each, grouped, grouped, grouped, grouped,
            pltpu.SemaphoreType.DMA((3,)),
        ],
        compiler_params=pltpu.CompilerParams(
            collective_id=0, has_side_effects=True, vmem_limit_bytes=60 * 1024 * 1024
        ),
    )(sendable, expert_gate, expert_up, expert_down)


def from_behind(value, axis, steps):
    count = lax.axis_size(axis)
    first, last = (max(0, -steps), min(count, count - steps))
    return lax.ppermute(value, axis, [(source, source + steps) for source in range(first, last)])


def swap(value, axis, offset):
    count = lax.axis_size(axis)
    return lax.ppermute(value, axis, [(source, source ^ offset) for source in range(count)])


def on_device(
    residual_in,
    conv_values,
    conv_gates,
    conv_kernel,
    conv_bias,
    chan_gain,
    chan_shift,
    out_weight,
    norm_gain,
    route_ids,
    route_weights,
    expert_gate,
    expert_up,
    expert_down,
):
    taps_count = conv_kernel.shape[0]
    tok_count, local_chan = conv_values.shape
    tp_count = lax.axis_size("tp")
    all_chan = local_chan * tp_count
    core = lax.axis_index("tp")
    gated = (
        conv_values.astype(jnp.float32) * jax.nn.sigmoid(conv_gates.astype(jnp.float32))
    ).astype(jnp.bfloat16)
    earlier = from_behind(gated[tok_count - (taps_count - 1) :], "sp", 1)
    extended = jnp.concatenate([earlier, gated], 0).astype(jnp.float32)
    mixed = jnp.zeros((tok_count, local_chan), jnp.float32) + conv_bias[None, :]
    for tap_index in range(taps_count):
        mixed = (
            mixed + conv_kernel[tap_index][None, :] * extended[tap_index : tap_index + tok_count]
        )
    sums = jnp.stack([jnp.sum(mixed, 1), jnp.sum(mixed * mixed, 1)])
    sums = sums + swap(sums, "tp", 1)
    center = (sums[0] / all_chan)[:, None]
    spread = (sums[1] / all_chan)[:, None] - center * center
    normed = (mixed - center) * lax.rsqrt(spread + 1e-06) * chan_gain[None, :] + chan_shift[None, :]
    activated = jax.nn.silu(normed).astype(jnp.bfloat16)
    row_count = tok_count // tp_count
    low, high = activated[:row_count], activated[row_count:]
    kept = jnp.where(core == 0, low, high)
    given = swap(jnp.where(core == 0, high, low), "tp", 1)
    regrouped = jnp.concatenate(
        [jnp.where(core == 0, kept, given), jnp.where(core == 0, given, kept)], 1
    )
    projected = jnp.dot(regrouped, out_weight, preferred_element_type=jnp.float32)
    after_f = (residual_in.astype(jnp.float32) + projected).astype(jnp.bfloat16).astype(jnp.float32)
    normal_rows = (
        after_f
        * lax.rsqrt(jnp.mean(after_f * after_f, 1, keepdims=True) + 1e-06)
        * norm_gain[None, :]
    ).astype(jnp.bfloat16)
    sp_count = lax.axis_size("sp")
    experts_all = expert_gate.shape[0] * sp_count
    choose_count = route_ids.shape[1]
    slot_cap = max(2, (2 * choose_count * row_count + experts_all - 1) // experts_all)
    slot_cap = (slot_cap + 15) // 16 * 16
    onehot = (
        route_ids.reshape(-1)[:, None] == jnp.arange(experts_all, dtype=jnp.int32)[None, :]
    ).astype(jnp.int32)
    before = jnp.cumsum(onehot, 0) - onehot
    ranking = jnp.sum(before * onehot, 1).reshape(row_count, choose_count)
    slot_ids = (route_ids ^ lax.axis_index("sp")) * slot_cap + ranking
    positions = lax.broadcasted_iota(jnp.int32, (experts_all * slot_cap, 1, 1), 0)
    dispatch = jnp.any(positions == slot_ids[None, :, :], axis=2).astype(jnp.bfloat16)
    columns = lax.broadcasted_iota(jnp.int32, (1, 1, experts_all * slot_cap), 2)
    weighting = jnp.sum(
        jnp.where(columns == slot_ids[:, :, None], route_weights[:, :, None], 0.0), 1
    )
    coarse_f = lax.reduce_precision(weighting, 8, 7)
    coarse = coarse_f.astype(jnp.bfloat16)
    fine = (weighting - coarse_f).astype(jnp.bfloat16)
    sendable = jnp.dot(dispatch, normal_rows, preferred_element_type=jnp.float32).astype(
        jnp.bfloat16
    )
    flat_out = run_experts(sendable, expert_gate, expert_up, expert_down, sp_count, slot_cap)
    combined = (
        after_f
        + jnp.dot(coarse, flat_out, preferred_element_type=jnp.float32)
        + jnp.dot(fine, flat_out, preferred_element_type=jnp.float32)
    )
    return combined.astype(jnp.bfloat16)


def solution(mesh):
    placed = (
        P(("sp", "tp"), None),
        P("sp", "tp"),
        P("sp", "tp"),
        P(None, "tp"),
        P("tp"),
        P("tp"),
        P("tp"),
        P(),
        P(),
        P(("sp", "tp"), None),
        P(("sp", "tp"), None),
        P("sp", None, "tp"),
        P("sp", None, "tp"),
        P("sp", "tp", None),
    )
    return jax.shard_map(
        on_device, mesh=mesh, in_specs=placed, out_specs=P(("sp", "tp"), None), check_vma=False
    )
```

time: 267 us -> 178 us (0.67)
  Pallas kernels: 0 us -> 147 us
  waiting for transfers between devices: 103 us -> 2.02 us
  blocking collectives: 82.3 us -> 0 us
  matrix products: 30.7 us -> 10.7 us
  between operations: 13.7 us -> 0.3 us
  local copies, waits for them, and re-layouts: 11.5 us -> 3.75 us
  other arithmetic: 14.8 us -> 7.16 us
  starting transfers between devices: 10.6 us -> 3.7 us
    pallas_call x0 -> x1, Pallas kernels: none -> 147 us  [run_experts(): pl.pallas_call(functools.partial(experts_kernel, count, cap), out_shape=j...]
    all_to_all x2 -> x0, blocking collectives: 79.7 us -> none  [the longest x1 75.6 us: on_device(): lax.all_to_all(sendable, 'sp', split_axis=0, concat_axis=0, tiled=True)]
    all_to_all x1 -> x0, waiting for transfers between devices: 69.5 us -> none  [on_device(): lax.all_to_all(summed, 'sp', split_axis=0, concat_axis=0, tiled=True)]
    dot_general x3 -> x2, matrix products: 26.3 us -> 4.54 us  [the longest x1 2.83 us: on_device(): jnp.dot(coarse, flat_out, preferred_element_type=jnp.float32)]
    all_gather x1 -> x0, waiting for transfers between devices: 16.9 us -> none  [on_device(): lax.all_gather(lax.all_to_all(sendable, 'sp', split_axis=0, concat_axis=0...]
    reduce_scatter x1 -> x0, waiting for transfers between devices: 16.2 us -> none  [on_device(): lax.psum_scatter(jnp.dot(hidden, expert_down[0], preferred_element_type=j...]
    all_to_all x1 -> x0, starting transfers between devices: 6.96 us -> none  [on_device(): lax.all_to_all(summed, 'sp', split_axis=0, concat_axis=0, tiled=True)]
    gather x2 -> x0, local copies, waits for them, and re-layouts: 6.02 us -> none  [on_device(): jnp.take(flat_out, slot_ids.reshape(-1), axis=0)]
  transfers between devices with their start and end apart: 4 -> 3, of which waited for: 3 -> 2; matrix products, arithmetic and copies ran while one was open for 2% -> 3% of each run, Pallas kernels for 0% -> 0%
where the time goes in v1:
time: 178 us; the launch traced here: 175 us
  Pallas kernels  147 us (83%)
  matrix products  10.7 us (6%)
  other arithmetic  7.16 us (4%)
  local copies, waits for them, and re-layouts  3.75 us (2%)
  starting transfers between devices  3.7 us (2%)
  waiting for transfers between devices  2.02 us (1%)
    pallas_call x1, Pallas kernels, run_experts(): pl.pallas_call(functools.partial(experts_kernel, count, cap), out_shape=j...  147 us
    reduce_sum x1, other arithmetic, on_device(): sums = jnp.stack([jnp.sum(mixed, 1), jnp.sum(mixed * mixed, 1)])  3.83 us
  transfers between devices with their start and end apart: 3, of which 2 were waited for; matrix products, arithmetic and copies ran while one was open for 3% of the time, Pallas kernels for 0%

profile of v1, /device:TPU:14, one launch (start us, length us, event | category | flops | bytes accessed | tf_op | source)
XLA Modules:
  0.0 175.1 jit_solution(1980439932750408297)
XLA Ops:
  0.0 0.0 copy-start.7
  0.0 1.4 multiply_convert_fusion.3
  1.4 3.4 %collective-permute-start = (bf16[30,512]{1,0:T(8,128)(2,1)S(1)}, bf16[30,512]{1,0:T(8,128)(2,1)S(1)}, u32[]{:S(2)}, u32[]{:S(2)}) collective-permute-start(bf16[30,512]{1,0:T(8,128)(2,1)S(1)} %slice.276), channel_id=1, source_target_pairs={{0,2},{2,4},{4,6},{6,8},{8,10},{10,12},{12,14},{14,16},{16,18},{18... | collective-permute-start | bytes 92168 | tf_op jit(solution)/shard_map/ppermute | solution.py:186
  4.8 1.1 fusion.52
  5.9 1.1 fusion.53
  7.0 0.8 copy.29
  7.8 0.1 eq.63
  7.9 0.1 eq.59
  8.1 0.9 reduce-window.6
  8.9 0.2 slice_reduce_fusion
  9.2 0.1 fusion.44
  9.3 0.1 reshape.61
  9.5 0.1 copy.32
  9.5 0.0 collective-permute-done
  9.5 0.1 maximum_convert_fusion
  9.7 0.0 copy-done.7
  9.7 0.0 copy-start.3
  9.7 0.0 copy-start.4
  9.7 0.0 copy-start.5
  9.7 3.8 %fusion.50 = (f32[384]{0:T(512)S(1)}, f32[384]{0:T(512)S(1)}, f32[384,512]{1,0:T(8,128)S(1)}) fusion(f32[414,512]{1,0:T(8,128)S(1)} %maximum_convert_fusion, f32[512]{0:T(512)S(1)} %bitcast.85, f32[512]{0:T(512)S(1)} %bitcast.86, f32[512]{0:T(512)S(1)} %bitcast.57, f32[512]{0:T(512)S(1)} %bitcast.58, f32[512]{0:T(512)S(1)} %bitcast.59, f32[512]{0:T(512)S(1)} %bitcast.60, ...), kind=kLoop, calls=%fused_computation.110 | loop fusion | flops 12778752 | bytes 25234432 | tf_op jit(solution)/shard_map/reduce_sum | solution.py:225
  13.5 0.0 copy-start.6
  13.6 0.1 collective-permute-start.1
  13.7 0.0 copy-done.3
  13.7 1.1 collective-permute-done.1
  14.9 0.0 copy-done.4
  14.9 0.0 copy-done.5
  14.9 0.0 copy-start.1
  14.9 0.4 multiply_convert_fusion.2
  15.3 0.2 collective-permute-start.2
  15.5 0.2 fusion.3
  15.7 0.0 copy-done.6
  15.7 0.2 select_reduce_fusion
  15.9 0.9 collective-permute-done.2
  16.9 0.0 copy-done.1
  16.9 0.0 copy-start.2
  16.9 3.4 %multiply_reduce_fusion = (f32[192]{0:T(256)S(1)}, f32[192,2048]{1,0:T(8,128)S(1)}) fusion(bf16[1024,2048]{1,0:T(8,128)(2,1)} %param.21, bf16[192,512]{1,0:T(8,128)(2,1)S(1)} %get-tuple-element.11, bf16[192,512]{1,0:T(8,128)(2,1)S(1)} %get-tuple-element.10, bf16[192,2048]{1,0:T(8,128)(2,1)S(1)} %copy-done.1), kind=kOutput, calls=%fused_computation.8 | convolution fusion | flops 808451904 | bytes 6947584 | tf_op jit(solution)/shard_map/dot_general | solution.py:238
  20.3 0.0 copy-done.2
  20.3 2.8 %convolution_convert_fusion.send = bf16[768,2048]{1,0:T(8,128)(2,1)} fusion(pred[768,192]{0,1:T(8,128)(4,1)S(1)} %fusion.3, f32[192,2048]{1,0:T(8,128)S(1)} %get-tuple-element.44, f32[2048]{0:T(1024)S(1)} %copy-done.2, f32[192]{0:T(256)S(1)} %add_rsqrt_fusion.1), kind=kOutput, calls=%fused_computation | convolution fusion | flops 606732288 | bytes 4875008 | tf_op jit(solution)/shard_map/dot_general | solution.py:265
  23.1 147.5 %shard_map.136 = bf16[768,2048]{1,0:T(8,128)(2,1)} custom-call(bf16[768,2048]{1,0:T(8,128)(2,1)} %convolution_convert_fusion.send, bf16[1,2048,1024]{2,1,0:T(8,128)(2,1)} %gate_in.1, bf16[1,2048,1024]{2,1,0:T(8,128)(2,1)} %up_in.1, bf16[1,1024,2048]{2,1,0:T(8,128)(2,1)} %down_in.1), custom_call_target="tpu_custom_call" | custom-call | tf_op jit(solution)/shard_map/pallas_call | solution.py:160
  170.6 0.0 copy-start
  170.6 2.8 %convolution_add_fusion.1 = f32[192,2048]{1,0:T(8,128)S(1)} fusion(f32[192,2048]{1,0:T(8,128)S(1)} %get-tuple-element.44, bf16[768,2048]{1,0:T(8,128)(2,1)} %shard_map.136, f32[192,768]{1,0:T(8,128)S(1)} %select_reduce_fusion), kind=kOutput, calls=%fused_computation.2 | convolution fusion | flops 604667904 | bytes 6881280 | tf_op jit(solution)/shard_map/dot_general | solution.py:271
  173.4 0.0 copy-done
  173.4 1.7 fusion.2
  (13 shorter events, 0.2 us)
Async XLA Ops:
  0.0 9.7 %copy-start.7 = (f32[512]{0:T(512)S(1)}, f32[512]{0:T(512)}, u32[]{:S(2)}) copy-start(f32[512]{0:T(512)} %param.18) | copy-start | bytes 6148
  1.4 8.2 %collective-permute-start = (bf16[30,512]{1,0:T(8,128)(2,1)S(1)}, bf16[30,512]{1,0:T(8,128)(2,1)S(1)}, u32[]{:S(2)}, u32[]{:S(2)}) collective-permute-start(bf16[30,512]{1,0:T(8,128)(2,1)S(1)} %slice.276), channel_id=1, source_target_pairs={{0,2},{2,4},{4,6},{6,8},{8,10},{10,12},{12,14},{14,16},{16,18},{18... | collective-permute-start | bytes 92168 | tf_op jit(solution)/shard_map/ppermute | solution.py:186
  9.7 4.0 %copy-start.3 = (s32[192,2]{0,1:T(2,128)S(1)}, s32[192,2]{0,1:T(2,128)}, u32[]{:S(2)}) copy-start(s32[192,2]{0,1:T(2,128)} %param.23) | copy-start | bytes 4612
  9.7 5.2 %copy-start.4 = (f32[512]{0:T(512)S(1)}, f32[512]{0:T(512)}, u32[]{:S(2)}) copy-start(f32[512]{0:T(512)} %param.20) | copy-start | bytes 6148
  9.7 5.2 %copy-start.5 = (f32[512]{0:T(512)S(1)}, f32[512]{0:T(512)}, u32[]{:S(2)}) copy-start(f32[512]{0:T(512)} %param.19) | copy-start | bytes 6148
  13.5 2.2 %copy-start.6 = (f32[192,2]{0,1:T(2,128)S(1)}, f32[192,2]{0,1:T(2,128)}, u32[]{:S(2)}) copy-start(f32[192,2]{0,1:T(2,128)} %param.24) | copy-start | bytes 4612
  13.6 1.2 collective-permute-start.1
  14.9 2.0 %copy-start.1 = (bf16[192,2048]{1,0:T(8,128)(2,1)S(1)}, bf16[192,2048]{1,0:T(8,128)(2,1)}, u32[]{:S(2)}) copy-start(bf16[192,2048]{1,0:T(8,128)(2,1)} %param.14) | copy-start | bytes 2359300
  15.3 1.5 collective-permute-start.2
  16.9 3.4 %copy-start.2 = (f32[2048]{0:T(1024)S(1)}, f32[2048]{0:T(1024)}, u32[]{:S(2)}) copy-start(f32[2048]{0:T(1024)} %param.22) | copy-start | bytes 24580
  170.6 2.8 %copy-start = (bf16[768,2048]{1,0:T(8,128)(2,1)S(1)}, bf16[768,2048]{1,0:T(8,128)(2,1)}, u32[]{:S(2)}) copy-start(bf16[768,2048]{1,0:T(8,128)(2,1)} %shard_map.136) | copy-start | bytes 9437188
